TPU v7x, 32 devices: a whole 2x2x4 slice. The times are simulated.
32 devices in a mesh: fs: 4 (over z), rep: 4 (over y, x), tp: 2 (over core).
Axes of the slice: x: 2, y: 2, z: 4, core: 2. Of those that a mesh axis runs over, the one named last changes fastest.
Arguments:
- input_act: bfloat16 [12288, 2048], P(('fs', 'rep')), may hold values from -6 to 6
- query_cot: bfloat16 [12288, 1024], P(('fs', 'rep'), 'tp'), may hold values from -6 to 6
- out_cot: bfloat16 [12288, 2048], P(('fs', 'rep')), may hold values from -6 to 6
- attn_out: bfloat16 [12288, 1024], P(('fs', 'rep'), 'tp'), may hold values from -6 to 6
- query_w: float32 [2048, 1024], P('fs', 'tp'), may hold values from -0.125 to 0.125
- out_w: float32 [1024, 2048], P('tp', 'fs'), may hold values from -0.1875 to 0.1875
- query_factor: bfloat16 [2048, 512], P('fs'), may hold values from -0.125 to 0.125
- out_factor: bfloat16 [2048, 512], P('fs'), may hold values from -0.125 to 0.125
- first_q: float32 [512, 1024], P('fs', 'tp'), may hold values from -6 to 6
- second_q: float32 [512, 1024], P('fs', 'tp'), may hold values from 0.075 to 120
- first_o: float32 [512, 1024], P('fs', 'tp'), may hold values from -6 to 6
- second_o: float32 [512, 1024], P('fs', 'tp'), may hold values from 0.075 to 120
Outputs:
- new_query_w: float32 [2048, 1024], P('fs', 'tp')
- new_out_w: float32 [1024, 2048], P('tp', 'fs')
- query_step: float32 [2048, 1024], P('fs', 'tp')
- out_step: float32 [1024, 2048], P('tp', 'fs')
- new_first_q: float32 [512, 1024], P('fs', 'tp')
- new_second_q: float32 [512, 1024], P('fs', 'tp')
- new_first_o: float32 [512, 1024], P('fs', 'tp')
- new_second_o: float32 [512, 1024], P('fs', 'tp')
- query_copy: bfloat16 [2048, 1024], P(None, 'tp')
- out_copy: bfloat16 [1024, 2048], P('tp')
All inputs are finite; a program needn't handle non-finite values.
Results may differ from a plain program's by a relative error of at most 0.0085.
Values may be sent and summed in bfloat16 or wider, within the bound.
A program may use at most 64 MiB of HBM per device.

v0:
```python
import math
import jax
import jax.numpy as jnp
from jax import lax
from jax.sharding import PartitionSpec as P

RANK = 512
HQ = 1024


def contract_rows(left_side, right_side):
    return lax.dot_general(
        left_side, right_side, (((0,), (0,)), ((), ())), preferred_element_type=jnp.float32
    )


def contract_exact(left_side, right_side):
    return lax.dot_general(
        left_side.astype(jnp.float32),
        right_side,
        (((0,), (0,)), ((), ())),
        precision=lax.Precision.HIGHEST,
        preferred_element_type=jnp.float32,
    )


def exact_dot(left_side, right_side):
    return jnp.dot(
        left_side, right_side, precision=lax.Precision.HIGHEST, preferred_element_type=jnp.float32
    )


def body(
    input_act,
    query_cot,
    out_cot,
    attn_out,
    query_w,
    out_w,
    query_factor,
    out_factor,
    first_q,
    second_q,
    first_o,
    second_o,
):
    heads_local = query_cot.shape[1]
    token_total = input_act.shape[0] * lax.axis_size("fs") * lax.axis_size("rep")
    scale_tokens = 1.0 / math.sqrt(token_total)
    gradient = lax.psum_scatter(
        jnp.concatenate(
            [contract_rows(input_act, query_cot), contract_rows(out_cot, attn_out)], axis=1
        ).astype(jnp.bfloat16),
        "fs",
        scatter_dimension=0,
        tiled=True,
    ).astype(jnp.float32)
    partial_value = jnp.concatenate(
        [
            contract_exact(query_factor, gradient[:, :heads_local]),
            contract_exact(out_factor, gradient[:, heads_local:]),
        ],
        axis=1,
    )
    projected = lax.psum_scatter(
        partial_value.astype(jnp.bfloat16), "fs", scatter_dimension=0, tiled=True
    ).astype(jnp.float32)
    projected = lax.psum(projected.astype(jnp.bfloat16), "rep").astype(jnp.float32) * scale_tokens
    proj_q = projected[:, :heads_local]
    proj_o = projected[:, heads_local:]
    new_first_q = 0.8 * first_q + 0.2 * proj_q
    new_second_q = 0.9 * second_q + 0.1 * proj_q * proj_q
    new_first_o = 0.8 * first_o + 0.2 * proj_o
    new_second_o = 0.9 * second_o + 0.1 * proj_o * proj_o
    dir_q = new_first_q / jnp.sqrt(new_second_q)
    dir_o = new_first_o / jnp.sqrt(new_second_o)
    local_squares = jnp.sum(dir_q * dir_q) + jnp.sum(dir_o * dir_o)
    total_squares = lax.psum(local_squares, ("fs", "tp"))
    norm_scale = jnp.sqrt(total_squares / (2 * RANK * HQ) + 1e-06)
    whole_dir_q, whole_dir_o = (
        lax.all_gather(dir_q, "fs", axis=0, tiled=True),
        lax.all_gather(dir_o, "fs", axis=0, tiled=True),
    )
    query_step = exact_dot(query_factor.astype(jnp.float32), whole_dir_q) / norm_scale
    out_step = (exact_dot(out_factor.astype(jnp.float32), whole_dir_o) / norm_scale).T
    new_query_w = query_w - 0.01 * query_step
    new_out_w = out_w - 0.01 * out_step
    query_copy = lax.all_gather(new_query_w.astype(jnp.bfloat16), "fs", axis=0, tiled=True)
    out_copy = lax.all_gather(new_out_w.astype(jnp.bfloat16), "fs", axis=1, tiled=True)
    return (
        new_query_w,
        new_out_w,
        query_step,
        out_step,
        new_first_q,
        new_second_q,
        new_first_o,
        new_second_o,
        query_copy,
        out_copy,
    )


def solution(mesh):
    return jax.shard_map(
        body,
        mesh=mesh,
        in_specs=(
            P(("fs", "rep"), None),
            P(("fs", "rep"), "tp"),
            P(("fs", "rep"), None),
            P(("fs", "rep"), "tp"),
            P("fs", "tp"),
            P("tp", "fs"),
            P("fs", None),
            P("fs", None),
            P("fs", "tp"),
            P("fs", "tp"),
            P("fs", "tp"),
            P("fs", "tp"),
        ),
        out_specs=(
            P("fs", "tp"),
            P("tp", "fs"),
            P("fs", "tp"),
            P("tp", "fs"),
            P("fs", "tp"),
            P("fs", "tp"),
            P("fs", "tp"),
            P("fs", "tp"),
            P(None, "tp"),
            P("tp", None),
        ),
        check_vma=False,
    )
```

profile of v0, /device:TPU:0, one launch (start us, length us, event | category | flops | bytes accessed | tf_op | source)
XLA Modules:
  0.0 343.3 jit_solution(11248011831809214401)
XLA Ops:
  7.2 1.8 copy-done
  9.1 3.1 convolution_convert_fusion.1
  12.2 1.9 convolution_convert_fusion
  14.1 2.5 pad_maximum_fusion
  16.8 79.6 %reduce-scatter.5.cloned.1.call-done = bf16[512,1024]{0,1:T(8,128)(2,1)} async-done(((bf16[2048,1024]{0,1:T(8,128)(2,1)}), bf16[512,1024]{0,1:T(8,128)(2,1)}) %reduce-scatter.5.cloned.1.call-update) | async-done | bytes 1048592 | tf_op jit(solution)/shard_map/reduce_scatter | solution.py:50
  100.7 2.3 copy.59
  103.0 27.9 %reduce-scatter.7.cloned.1.call-done = bf16[128,1024]{1,0:T(8,128)(2,1)} async-done(((bf16[512,1024]{1,0:T(8,128)(2,1)}), bf16[128,1024]{1,0:T(8,128)(2,1)}) %reduce-scatter.7.cloned.1.call-update) | async-done | bytes 262160
  139.0 37.0 %all-reduce.2.cloned.1.call-done = bf16[128,1024]{0,1:T(8,128)(2,1)} async-done(((bf16[128,1024]{0,1:T(8,128)(2,1)}), bf16[128,1024]{0,1:T(8,128)(2,1)}) %all-reduce.2.cloned.1.call-update) | async-done | bytes 262160 | tf_op jit(solution)/shard_map/psum | solution.py:68
  177.0 2.9 multiply_reduce_fusion
  181.9 2.5 copy.45
  184.4 16.9 %psum.15 = f32[]{:T(128)} all-reduce(f32[]{:T(128)S(6)} %add.30), channel_id=1, replica_groups=mesh['fs'=4,'rep'=4,'tp'=2] {'fs','tp'}, use_global_device_ids=true, to_apply=%region_5.0 | all-reduce | flops 1 | bytes 8 | tf_op jit(solution)/shard_map/psum | solution.py:78
  202.0 8.3 %all-gather.5.cloned.1.call-done = f32[512,512]{0,1:T(8,128)} async-done(((f32[128,512]{0,1:T(8,128)}), f32[512,512]{0,1:T(8,128)}) %all-gather.5.cloned.1.call-update) | async-done | bytes 1048592 | tf_op jit(solution)/shard_map/all_gather | solution.py:81
  210.3 4.2 %fusion.8 = (bf16[512,512]{0,1:T(8,128)(2,1)}, f32[512,512]{0,1:T(8,128)}, f32[512,512]{0,1:T(8,128)}) fusion(f32[512,512]{0,1:T(8,128)} %copy.45, f32[]{:T(128)S(6)} %sqrt.11, f32[512,512]{0,1:T(8,128)} %all-gather.5.cloned.1.call-done, bf16[512,512]{1,0:T(8,128)(2,1)} %param.18), kind=kOutput, calls=%fused_computation.27 | convolution fusion | flops 1611661312 | bytes 5242884 | tf_op jit(solution)/shard_map/dot_general | solution.py:28
  214.6 2.5 copy.47
  217.1 23.4 %all-gather.7.cloned.1.call-done = f32[512,512]{0,1:T(8,128)} async-done(((f32[128,512]{0,1:T(8,128)}), f32[512,512]{0,1:T(8,128)}) %all-gather.7.cloned.1.call-update) | async-done | bytes 1048592 | tf_op jit(solution)/shard_map/all_gather | solution.py:82
  240.5 4.3 %fusion.7 = (bf16[512,512]{0,1:T(8,128)(2,1)}, f32[512,512]{0,1:T(8,128)}, f32[512,512]{0,1:T(8,128)}) fusion(f32[512,512]{0,1:T(8,128)} %copy.47, f32[]{:T(128)S(6)} %sqrt.11, f32[512,512]{0,1:T(8,128)} %all-gather.7.cloned.1.call-done, bf16[512,512]{1,0:T(8,128)(2,1)} %param.19), kind=kOutput, calls=%fused_computation.26 | convolution fusion | flops 1611661312 | bytes 5242884 | tf_op jit(solution)/shard_map/dot_general | solution.py:28
  251.1 2.5 copy.49
  253.6 2.5 copy.51
  256.1 2.5 copy.48
  258.7 2.5 copy.50
  261.2 25.3 %all-gather.9.cloned.1.call-done = bf16[2048,512]{0,1:T(8,128)(2,1)} async-done(((bf16[512,512]{0,1:T(8,128)(2,1)}), bf16[2048,512]{0,1:T(8,128)(2,1)}) %all-gather.9.cloned.1.call-update) | async-done | bytes 2097168 | tf_op jit(solution)/shard_map/all_gather | solution.py:88
  286.5 3.9 %copy.56 = bf16[2048,512]{1,0:T(8,128)(2,1)} copy(bf16[2048,512]{0,1:T(8,128)(2,1)} %all-gather.9.cloned.1.call-done) | data formatting | bytes 4194304
  290.4 42.1 %all-gather.11.cloned.1.call-done = bf16[512,2048]{0,1:T(8,128)(2,1)} async-done(((bf16[512,512]{0,1:T(8,128)(2,1)}), bf16[512,2048]{0,1:T(8,128)(2,1)}) %all-gather.11.cloned.1.call-update) | async-done | bytes 2097168 | tf_op jit(solution)/shard_map/all_gather | solution.py:89
  332.6 3.9 %copy.57 = bf16[512,2048]{1,0:T(8,128)(2,1)} copy(bf16[512,2048]{0,1:T(8,128)(2,1)} %all-gather.11.cloned.1.call-done) | data formatting | bytes 4194304
  (34 shorter events, 20.4 us)
Async XLA Ops:
  7.2 1.9 copy-start
  7.2 89.2 %reduce-scatter.5.cloned.1.call-start = ((), (), s32[]{:S(2)}) async-start(), calls=%async_computation.2 | async-start | bytes 5242880 | tf_op jit(solution)/shard_map/reduce_scatter | solution.py:50
  9.1 3.1 copy-start.2
  9.1 3.1 copy-start.3
  16.7 114.2 %reduce-scatter.7.cloned.1.call-start = ((), (), s32[]{:S(2)}) async-start(), calls=%async_computation.8 | async-start | bytes 1310720
  99.7 33.2 %copy-start.1 = (f32[128,512]{1,0:T(8,128)S(1)}, f32[128,512]{1,0:T(8,128)}, u32[]{:S(2)}) copy-start(f32[128,512]{1,0:T(8,128)} %param.20) | copy-start | bytes 786436
  103.0 73.0 %all-reduce.2.cloned.1.call-start = ((), (), s32[]{:S(2)}) async-start(), calls=%async_computation.3 | async-start | bytes 524288 | tf_op jit(solution)/shard_map/psum | solution.py:68
  132.8 77.5 %all-gather.5.cloned.1.call-start = ((), (), s32[]{:S(2)}) async-start(), calls=%async_computation.4 | async-start | bytes 1310720 | tf_op jit(solution)/shard_map/all_gather | solution.py:81
  179.9 60.6 %all-gather.7.cloned.1.call-start = ((), (), s32[]{:S(2)}) async-start(), calls=%async_computation.5 | async-start | bytes 1310720 | tf_op jit(solution)/shard_map/all_gather | solution.py:82
  180.5 106.0 %all-gather.9.cloned.1.call-start = ((), (), s32[]{:S(2)}) async-start(), calls=%async_computation.6 | async-start | bytes 2621440 | tf_op jit(solution)/shard_map/all_gather | solution.py:88
  214.6 118.0 %all-gather.11.cloned.1.call-start = ((), (), s32[]{:S(2)}) async-start(), calls=%async_computation.7 | async-start | bytes 2621440 | tf_op jit(solution)/shard_map/all_gather | solution.py:89
Sparse Core Ops, SparseCore 0:
  16.8 79.5 reduce-scatter.4
  103.1 27.7 reduce-scatter.6
  134.4 41.5 all-reduce.1
  180.1 30.1 all-gather.4
  212.3 28.2 all-gather.6
  242.5 43.9 all-gather.8
  288.1 44.4 all-gather.10
where the time goes:
time: 344 us; the launch traced here: 343 us
  waiting for transfers between devices  244 us (71%)
  local copies, waits for them, and re-layouts  41.3 us (12%)
  blocking collectives  16.9 us (5%)
  matrix products  16.8 us (5%)
  between operations  16.2 us (5%)
  other arithmetic  7.46 us (2%)
    reduce_scatter x1, waiting for transfers between devices, body(): lax.psum_scatter(jnp.concatenate([contract_rows(input_act, query_cot), co...  79.6 us
    all_gather x1, waiting for transfers between devices, body(): lax.all_gather(new_out_w.astype(jnp.bfloat16), 'fs', axis=1, tiled=True)  42.1 us
    unnamed x26, local copies, waits for them, and re-layouts  41.3 us
    psum x1, waiting for transfers between devices, body(): lax.psum(projected.astype(jnp.bfloat16), 'rep').astype(jnp.float32)  37 us
    unnamed x8, waiting for transfers between devices  28.5 us
    all_gather x1, waiting for transfers between devices, body(): lax.all_gather(new_query_w.astype(jnp.bfloat16), 'fs', axis=0, tiled=True)  25.3 us
    all_gather x1, waiting for transfers between devices, body(): lax.all_gather(dir_o, 'fs', axis=0, tiled=True)  23.4 us
    psum x1, blocking collectives, body(): total_squares = lax.psum(local_squares, ('fs', 'tp'))  16.9 us
  transfers between devices with their start and end apart: 7, of which 7 were waited for; matrix products, arithmetic and copies ran while one was open for 12% of the time, Pallas kernels for 0%

commit v1 on v0

--- a/solution.py
+++ b/solution.py
@@ -85,7 +85,9 @@
     out_step = (exact_dot(out_factor.astype(jnp.float32), whole_dir_o) / norm_scale).T
     new_query_w = query_w - 0.01 * query_step
     new_out_w = out_w - 0.01 * out_step
-    query_copy = lax.all_gather(new_query_w.astype(jnp.bfloat16), "fs", axis=0, tiled=True)
+    x = new_query_w.astype(jnp.bfloat16)
+    sent = jnp.stack([x] * lax.axis_size("fs"))
+    query_copy = jnp.concatenate(lax.all_to_all(sent, "fs", 0, 0), axis=0)
     out_copy = lax.all_gather(new_out_w.astype(jnp.bfloat16), "fs", axis=1, tiled=True)
     return (
         new_query_w,

time: 344 us -> 340 us (0.988)
  waiting for transfers between devices: 244 us -> 232 us
  starting transfers between devices: 0.29 us -> 4.7 us
  local copies, waits for them, and re-layouts: 41.3 us -> 45 us
    all_gather x1 -> x0, waiting for transfers between devices: 25.3 us -> none  [body(): lax.all_gather(new_query_w.astype(jnp.bfloat16), 'fs', axis=0, tiled=True)]
    all_gather x1, waiting for transfers between devices: 23.4 us -> 35.9 us  [body(): lax.all_gather(dir_o, 'fs', axis=0, tiled=True)]
    all_to_all x0 -> x1, waiting for transfers between devices: none -> 4.56 us  [body(): query_copy = jnp.concatenate(lax.all_to_all(sent, 'fs', 0, 0), axis=0)]
    all_to_all x0 -> x1, starting transfers between devices: none -> 4.45 us  [body(): query_copy = jnp.concatenate(lax.all_to_all(sent, 'fs', 0, 0), axis=0)]
    unnamed x8 -> x7, waiting for transfers between devices: 28.5 us -> 28.5 us
where the time goes in v1:
time: 340 us; the launch traced here: 339 us
  waiting for transfers between devices  232 us (68%)
  local copies, waits for them, and re-layouts  45 us (13%)
  blocking collectives  17 us (5%)
  matrix products  16.9 us (5%)
  between operations  16.2 us (5%)
  other arithmetic  7.5 us (2%)
  starting transfers between devices  4.7 us (1%)
    reduce_scatter x1, waiting for transfers between devices, body(): lax.psum_scatter(jnp.concatenate([contract_rows(input_act, query_cot), co...  79.6 us
    all_gather x1, waiting for transfers between devices, body(): lax.all_gather(new_out_w.astype(jnp.bfloat16), 'fs', axis=1, tiled=True)  40.5 us
    unnamed x26, local copies, waits for them, and re-layouts  40.4 us
    psum x1, waiting for transfers between devices, body(): lax.psum(projected.astype(jnp.bfloat16), 'rep').astype(jnp.float32)  37 us
    all_gather x1, waiting for transfers between devices, body(): lax.all_gather(dir_o, 'fs', axis=0, tiled=True)  35.9 us
    unnamed x7, waiting for transfers between devices  28.5 us
    psum x1, blocking collectives, body(): total_squares = lax.psum(local_squares, ('fs', 'tp'))  17 us
    dot_general x2, matrix products, exact_dot(): jnp.dot(left_side, right_side, precision=lax.Precision.HIGHEST, preferred...  8.55 us
  transfers between devices with their start and end apart: 7, of which 7 were waited for; matrix products, arithmetic and copies ran while one was open for 12% of the time, Pallas kernels for 0%

profile of v1, /device:TPU:0, one launch (start us, length us, event | category | flops | bytes accessed | tf_op | source)
XLA Modules:
  0.0 339.1 jit_solution(16285674474355395679)
XLA Ops:
  9.1 3.1 convolution_convert_fusion
  14.1 2.5 pad_maximum_fusion
  16.8 79.6 %reduce-scatter.5.cloned.1.call-done = bf16[512,1024]{0,1:T(8,128)(2,1)} async-done(((bf16[2048,1024]{0,1:T(8,128)(2,1)}), bf16[512,1024]{0,1:T(8,128)(2,1)}) %reduce-scatter.5.cloned.1.call-update) | async-done | bytes 1048592 | tf_op jit(solution)/shard_map/reduce_scatter | solution.py:50
  100.7 2.3 copy.59
  103.0 27.9 %reduce-scatter.7.cloned.1.call-done = bf16[128,1024]{1,0:T(8,128)(2,1)} async-done(((bf16[512,1024]{1,0:T(8,128)(2,1)}), bf16[128,1024]{1,0:T(8,128)(2,1)}) %reduce-scatter.7.cloned.1.call-update) | async-done | bytes 262160
  139.0 37.0 %all-reduce.2.cloned.1.call-done = bf16[128,1024]{0,1:T(8,128)(2,1)} async-done(((bf16[128,1024]{0,1:T(8,128)(2,1)}), bf16[128,1024]{0,1:T(8,128)(2,1)}) %all-reduce.2.cloned.1.call-update) | async-done | bytes 262160 | tf_op jit(solution)/shard_map/psum | solution.py:68
  177.0 2.9 multiply_reduce_fusion
  180.6 2.5 copy.45
  184.4 2.5 copy.47
  186.9 17.0 %psum.15 = f32[]{:T(128)} all-reduce(f32[]{:T(128)S(6)} %add.30), channel_id=1, replica_groups=mesh['fs'=4,'rep'=4,'tp'=2] {'fs','tp'}, use_global_device_ids=true, to_apply=%region_5.0 | all-reduce | flops 1 | bytes 8 | tf_op jit(solution)/shard_map/psum | solution.py:78
  204.6 5.7 %all-gather.4.cloned.1.call-done = f32[512,512]{0,1:T(8,128)} async-done(((f32[128,512]{0,1:T(8,128)}), f32[512,512]{0,1:T(8,128)}) %all-gather.4.cloned.1.call-update) | async-done | bytes 1048592 | tf_op jit(solution)/shard_map/all_gather | solution.py:81
  210.3 4.2 %fusion.8 = (bf16[512,512]{0,1:T(8,128)(2,1)}, f32[512,512]{0,1:T(8,128)}, f32[512,512]{0,1:T(8,128)}) fusion(f32[512,512]{0,1:T(8,128)} %copy.45, f32[]{:T(128)S(6)} %sqrt.11, f32[512,512]{0,1:T(8,128)} %all-gather.4.cloned.1.call-done, bf16[512,512]{1,0:T(8,128)(2,1)} %param.18), kind=kOutput, calls=%fused_computation.27 | convolution fusion | flops 1611661312 | bytes 5242884 | tf_op jit(solution)/shard_map/dot_general | solution.py:28
  216.6 2.5 stack.2
  219.1 4.5 %all-to-all-start = ((bf16[4,512,512]{2,1,0:T(8,128)(2,1)}), bf16[4,512,512]{2,1,0:T(8,128)(2,1)}, u32[]{:S(2)}, u32[]{:S(2)}) async-start(bf16[4,512,512]{2,1,0:T(8,128)(2,1)} %stack.2), calls=%async_computation.1 | async-start | bytes 4194304 | tf_op jit(solution)/shard_map/all_to_all | solution.py:90
  223.6 35.9 %all-gather.6.cloned.1.call-done = f32[512,512]{0,1:T(8,128)} async-done(((f32[128,512]{0,1:T(8,128)}), f32[512,512]{0,1:T(8,128)}) %all-gather.6.cloned.1.call-update) | async-done | bytes 1048592 | tf_op jit(solution)/shard_map/all_gather | solution.py:82
  259.6 4.3 %fusion.7 = (bf16[512,512]{0,1:T(8,128)(2,1)}, f32[512,512]{0,1:T(8,128)}, f32[512,512]{0,1:T(8,128)}) fusion(f32[512,512]{0,1:T(8,128)} %copy.47, f32[]{:T(128)S(6)} %sqrt.11, f32[512,512]{0,1:T(8,128)} %all-gather.6.cloned.1.call-done, bf16[512,512]{1,0:T(8,128)(2,1)} %param.19), kind=kOutput, calls=%fused_computation.26 | convolution fusion | flops 1611661312 | bytes 5242884 | tf_op jit(solution)/shard_map/dot_general | solution.py:28
  270.1 2.5 copy.49
  272.6 2.5 copy.50
  275.2 2.5 copy.51
  277.7 2.5 copy.52
  280.2 4.6 %all-to-all-done = bf16[4,512,512]{2,1,0:T(8,128)(2,1)} async-done(((bf16[4,512,512]{2,1,0:T(8,128)(2,1)}), bf16[4,512,512]{2,1,0:T(8,128)(2,1)}, u32[]{:S(2)}, u32[]{:S(2)}) %all-to-all-start) | async-done | bytes 2097184 | tf_op jit(solution)/shard_map/all_to_all | solution.py:90
  284.8 40.5 %all-gather.8.cloned.1.call-done = bf16[512,2048]{0,1:T(8,128)(2,1)} async-done(((bf16[512,512]{0,1:T(8,128)(2,1)}), bf16[512,2048]{0,1:T(8,128)(2,1)}) %all-gather.8.cloned.1.call-update) | async-done | bytes 2097168 | tf_op jit(solution)/shard_map/all_gather | solution.py:91
  325.3 3.9 %copy.57 = bf16[512,2048]{1,0:T(8,128)(2,1)} copy(bf16[512,2048]{0,1:T(8,128)(2,1)} %all-gather.8.cloned.1.call-done) | data formatting | bytes 4194304
  329.2 3.0 copy.63
  (35 shorter events, 26.1 us)
Async XLA Ops:
  7.2 1.9 copy-start
  7.2 89.2 %reduce-scatter.5.cloned.1.call-start = ((), (), s32[]{:S(2)}) async-start(), calls=%async_computation.3 | async-start | bytes 5242880 | tf_op jit(solution)/shard_map/reduce_scatter | solution.py:50
  9.1 3.1 copy-start.2
  9.1 3.1 copy-start.3
  16.7 114.2 %reduce-scatter.7.cloned.1.call-start = ((), (), s32[]{:S(2)}) async-start(), calls=%async_computation.8 | async-start | bytes 1310720
  99.7 33.2 %copy-start.1 = (f32[128,512]{1,0:T(8,128)S(1)}, f32[128,512]{1,0:T(8,128)}, u32[]{:S(2)}) copy-start(f32[128,512]{1,0:T(8,128)} %param.23) | copy-start | bytes 786436
  103.0 73.0 %all-reduce.2.cloned.1.call-start = ((), (), s32[]{:S(2)}) async-start(), calls=%async_computation.4 | async-start | bytes 524288 | tf_op jit(solution)/shard_map/psum | solution.py:68
  132.8 77.6 %all-gather.4.cloned.1.call-start = ((), (), s32[]{:S(2)}) async-start(), calls=%async_computation.5 | async-start | bytes 1310720 | tf_op jit(solution)/shard_map/all_gather | solution.py:81
  180.0 79.6 %all-gather.6.cloned.1.call-start = ((), (), s32[]{:S(2)}) async-start(), calls=%async_computation.6 | async-start | bytes 1310720 | tf_op jit(solution)/shard_map/all_gather | solution.py:82
  219.1 65.7 %all-to-all-start = ((bf16[4,512,512]{2,1,0:T(8,128)(2,1)}), bf16[4,512,512]{2,1,0:T(8,128)(2,1)}, u32[]{:S(2)}, u32[]{:S(2)}) async-start(bf16[4,512,512]{2,1,0:T(8,128)(2,1)} %stack.2), calls=%async_computation.1 | async-start | bytes 4194304 | tf_op jit(solution)/shard_map/all_to_all | solution.py:90
  223.6 101.7 %all-gather.8.cloned.1.call-start = ((), (), s32[]{:S(2)}) async-start(), calls=%async_computation.7 | async-start | bytes 2621440 | tf_op jit(solution)/shard_map/all_gather | solution.py:91
Sparse Core Ops, SparseCore 0:
  16.8 79.5 reduce-scatter.4
  103.1 27.7 reduce-scatter.6
  134.4 41.5 all-reduce.1
  180.1 30.1 all-gather.3
  212.3 47.2 all-gather.5
  264.0 61.2 all-gather.7
